TPU v7x, 32 devices: a whole 2x2x4 slice. The times are simulated.
32 devices in a mesh: sp: 8 (over z, y), tp: 4 (over x, core).
Axes of the slice: x: 2, y: 2, z: 4, core: 2. Of those that a mesh axis runs over, the one named last changes fastest.
Arguments:
- tokens: bfloat16 [4, 1024, 2048], P(None, 'sp'), may hold values from -6 to 6
- next_tokens: bfloat16 [4, 2048], replicated, may hold values from -6 to 6
- w_query: bfloat16 [2048, 2048], P(None, 'tp'), may hold values from -0.125 to 0.125
- w_key: bfloat16 [2048, 2048], P(None, 'tp'), may hold values from -0.125 to 0.125
- w_value: bfloat16 [2048, 2048], P(None, 'tp'), may hold values from -0.125 to 0.125
- w_in_gate: bfloat16 [2048, 8], replicated, may hold values from -0.125 to 0.125
- w_forget_gate: bfloat16 [2048, 8], replicated, may hold values from -0.125 to 0.125
- forget_bias: float32 [8], replicated, may hold values from 3 to 14
- extra_decay: float32 [8, 4, 1024], P('tp', None, 'sp'), may hold values from -0.5509766 to 0
- w_out: bfloat16 [2048, 2048], P('tp'), may hold values from -0.125 to 0.125
Outputs:
- memory: bfloat16 [8, 1024, 256], P('tp', 'sp')
- normalizer: float32 [8, 1024], P('tp', 'sp')
- stabilizer: float32 [4, 8], P(None, 'tp')
- read: bfloat16 [4, 2048], replicated
All inputs are finite; a program needn't handle non-finite values.
Results may differ from a plain program's by a relative error of at most 0.024.
Values may be sent and summed in bfloat16 or wider, within the bound.
A program may use at most 64 MiB of HBM per device.

v0:
```python
import jax
import jax.numpy as jnp
from jax import lax
from jax.sharding import PartitionSpec as P

HD = 256


def per_device(
    tokens,
    next_tokens,
    w_query,
    w_key,
    w_value,
    w_in_gate,
    w_forget_gate,
    forget_bias,
    extra_decay,
    w_out,
):
    scale = HD ** (-0.5)
    seq_count = tokens.shape[0]
    span = tokens.shape[1]
    heads_here = w_key.shape[1] // HD
    sp_size = lax.axis_size("sp")
    sp_index = lax.axis_index("sp")
    head_start = lax.axis_index("tp") * heads_here
    gate_in = lax.dynamic_slice_in_dim(w_in_gate, head_start, heads_here, 1)
    gate_forget = lax.dynamic_slice_in_dim(w_forget_gate, head_start, heads_here, 1)
    bias_here = lax.dynamic_slice_in_dim(forget_bias, head_start, heads_here, 0)
    flat = tokens.reshape(seq_count * span, tokens.shape[2])
    keys = jnp.dot(flat, w_key, preferred_element_type=jnp.float32).astype(jnp.bfloat16)
    values = jnp.dot(flat, w_value, preferred_element_type=jnp.float32).astype(jnp.bfloat16)
    log_in = jnp.dot(flat, gate_in, preferred_element_type=jnp.float32).reshape(
        seq_count, span, heads_here
    )
    log_forget = jax.nn.log_sigmoid(
        jnp.dot(flat, gate_forget, preferred_element_type=jnp.float32) + bias_here
    ).reshape(seq_count, span, heads_here) + jnp.transpose(extra_decay, (1, 2, 0))
    prefix = jnp.cumsum(log_forget, axis=1)
    block_total = prefix[:, -1]
    local_score = block_total[:, None, :] - prefix + log_in
    block_peak = jnp.max(local_score, axis=1)
    totals, peaks = (
        lax.all_gather(block_total[None], "sp", axis=0, tiled=True),
        lax.all_gather(block_peak[None], "sp", axis=0, tiled=True),
    )
    later = jnp.flip(jnp.cumsum(jnp.flip(totals, 0), axis=0), 0) - totals
    prompt_total = jnp.sum(totals, axis=0)
    stabilizer = jnp.maximum(prompt_total, jnp.max(later + peaks, axis=0))
    pick_block = (jnp.arange(sp_size) == sp_index).astype(jnp.float32)
    later_here = jnp.sum(pick_block[:, None, None] * later, axis=0)
    weight = jnp.exp(later_here[:, None, :] + local_score - stabilizer[:, None, :]) * scale
    key_heads = keys.reshape(seq_count, span, heads_here, HD)
    value_heads = values.reshape(seq_count, span, heads_here, HD)
    weighted = (key_heads.astype(jnp.float32) * weight[:, :, :, None]).astype(jnp.bfloat16)
    block_memory = jnp.einsum(
        "sthd,sthe->hsde", weighted, value_heads, preferred_element_type=jnp.float32
    )
    block_norm = jnp.transpose(jnp.sum(weighted.astype(jnp.float32), axis=1), (1, 0, 2))
    memory_term = block_memory.reshape(heads_here, seq_count * HD, HD)
    norm_term = block_norm.reshape(heads_here, seq_count * HD)
    memory_rows, norm_rows = (
        lax.psum_scatter(memory_term, "sp", scatter_dimension=1, tiled=True),
        lax.psum_scatter(norm_term, "sp", scatter_dimension=1, tiled=True),
    )
    query = (
        jnp.dot(next_tokens, w_query, preferred_element_type=jnp.float32)
        .astype(jnp.bfloat16)
        .astype(jnp.float32)
        .reshape(seq_count, heads_here, HD)
    )
    new_key = (
        jnp.dot(next_tokens, w_key, preferred_element_type=jnp.float32)
        .astype(jnp.bfloat16)
        .astype(jnp.float32)
        .reshape(seq_count, heads_here, HD)
        * scale
    )
    new_value = (
        jnp.dot(next_tokens, w_value, preferred_element_type=jnp.float32)
        .astype(jnp.bfloat16)
        .astype(jnp.float32)
        .reshape(seq_count, heads_here, HD)
    )
    new_in = jnp.dot(next_tokens, gate_in, preferred_element_type=jnp.float32)
    new_forget = jax.nn.log_sigmoid(
        jnp.dot(next_tokens, gate_forget, preferred_element_type=jnp.float32) + bias_here
    )
    numer_slots = jnp.einsum("shd,hsde->she", query, block_memory, precision=lax.Precision.HIGHEST)
    denom_slots = jnp.einsum("shd,hsd->sh", query, block_norm, precision=lax.Precision.HIGHEST)
    query_state, query_norm = lax.psum((numer_slots, denom_slots), "sp")
    top = jnp.maximum(new_forget + stabilizer, new_in)
    keep = jnp.exp(new_forget + stabilizer - top)
    take = jnp.exp(new_in - top)
    qk = jnp.sum(query * new_key, axis=-1)
    numer = keep[:, :, None] * query_state + (take * qk)[:, :, None] * new_value
    denom = keep * query_norm + take * qk
    head_out = (numer / jnp.maximum(jnp.abs(denom), 1.0)[:, :, None]).astype(jnp.bfloat16)
    partial_value = (
        jnp.dot(
            head_out.reshape(seq_count, heads_here * HD), w_out, preferred_element_type=jnp.float32
        )
        .astype(jnp.bfloat16)
        .astype(jnp.float32)
    )
    read = lax.psum(partial_value.astype(jnp.bfloat16), "tp")
    return (memory_rows.astype(jnp.bfloat16), norm_rows, stabilizer, read)


def solution(mesh):
    placed = (
        P(None, "sp", None),
        P(),
        P(None, "tp"),
        P(None, "tp"),
        P(None, "tp"),
        P(),
        P(),
        P(),
        P("tp", None, "sp"),
        P("tp", None),
    )
    return jax.shard_map(
        per_device,
        mesh=mesh,
        in_specs=placed,
        out_specs=(P("tp", "sp", None), P("tp", "sp"), P(None, "tp"), P()),
        check_vma=False,
    )
```

profile of v0, /device:TPU:0, one launch (start us, length us, event | category | flops | bytes accessed | tf_op | source)
XLA Modules:
  0.0 210.3 jit_solution(8536744384994718266)
XLA Ops:
  7.2 0.0 copy-start
  7.2 0.0 copy-start.2
  7.2 0.0 reduce-scatter.7.cloned.1.call-start
  7.2 0.9 dynamic_slice.10
  8.1 0.7 copy-done
  8.8 1.4 fusion.16
  10.2 0.0 copy-done.2
  10.3 0.1 copy.40
  10.4 0.3 reduce_window_sum.22
  10.7 27.9 %all-gather = f32[32,1,2]{2,1,0:T(1,128)S(1)} all-gather(f32[4,1,2]{2,1,0:T(1,128)S(1)} %slice.4), channel_id=2, replica_groups=mesh['sp'=8,'tp'=4] {'sp'}, dimensions={0}, use_global_device_ids=true | all-gather | bytes 288 | tf_op jit(solution)/shard_map/all_gather | solution.py:45
  38.6 0.1 copy.63
  38.8 2.8 %fusion.2 = f32[512,512]{1,0:T(8,128)S(1)} fusion(bf16[512,2048]{1,0:T(8,128)(2,1)S(1)} %bitcast.53, bf16[2048,512]{1,0:T(8,128)(2,1)} %param.13), kind=kOutput, calls=%fused_computation.5 | convolution fusion | flops 1074266112 | bytes 5242880 | tf_op jit(solution)/shard_map/dot_general | solution.py:32
  41.6 0.0 copy-start.4
  41.6 1.6 reshape.82
  43.3 1.5 copy.50
  44.7 0.1 copy.69
  44.9 0.0 copy-done.4
  44.9 0.6 convolution_bitcast_fusion
  45.5 0.9 copy.65
  46.4 1.0 fusion.13
  47.4 0.1 copy.46
  47.5 19.0 %all-gather.2 = f32[8,4,2]{1,2,0:T(2,128)S(1)} all-gather(f32[1,4,2]{1,2,0:T(2,128)S(1)} %bitcast.68), channel_id=3, replica_groups=mesh['sp'=8,'tp'=4] {'sp'}, dimensions={0}, use_global_device_ids=true | all-gather | bytes 288 | tf_op jit(solution)/shard_map/all_gather | solution.py:46
  66.5 0.1 multiply_reduce_fusion.1
  66.6 0.0 copy-start.3
  66.6 0.1 copy.48
  66.7 0.1 copy.42
  66.8 1.7 exponential_multiply_fusion
  68.5 1.1 copy.49
  69.5 0.4 convert_reduce_fusion
  69.9 1.0 copy.68
  70.9 0.0 reduce-scatter.7.cloned.1.call-update
  71.0 0.0 reduce-scatter.5.cloned.1.call-start
  71.0 3.6 %convolution_convert_fusion.1 = bf16[512,512]{1,0:T(8,128)(2,1)} fusion(bf16[512,2048]{1,0:T(8,128)(2,1)S(1)} %bitcast.56, bf16[2048,512]{1,0:T(8,128)(2,1)} %param.14), kind=kOutput, calls=%fused_computation.3 | convolution fusion | flops 1074003968 | bytes 4718592 | tf_op jit(solution)/shard_map/dot_general | solution.py:33
  74.6 2.0 reshape.75
  76.6 0.0 copy-start.1
  76.6 2.8 %fusion.11 = f32[2,4,256,256]{3,2,1,0:T(8,128)} fusion(bf16[4,128,2,256]{3,2,1,0:T(2,128)(2,1)} %reshape.75, f32[4,128,2,256]{1,3,0,2:T(8,128)S(1)} %copy.50, f32[4,128,2]{1,0,2:T(4,128)S(1)} %copy.49), kind=kOutput, calls=%fused_computation.23 | convolution fusion | flops 134742016 | bytes 3674112 | tf_op jit(solution)/shard_map/sthd,sthe->hsde/dot_general | solution.py:57
  79.5 0.0 reduce-scatter.5.cloned.1.call-update
  79.5 0.0 copy-done.1
  79.5 2.0 convolution_convert_fusion.5
  81.5 2.4 %fusion = f32[4,2,1,256]{3,2,1,0:T(1,128)S(1)} fusion(bf16[4,2,256,1]{2,3,1,0:T(2,128)(2,1)S(1)} %reshape.95, f32[2,4,256,256]{3,2,1,0:T(8,128)} %fusion.11), kind=kOutput, calls=%fused_computation.1 | convolution fusion | flops 6291456 | bytes 2109440 | tf_op jit(solution)/shard_map/shd,hsde->she/dot_general | solution.py:90
  83.9 0.1 multiply_reduce_fusion
  84.0 17.7 %all-reduce = (f32[4,2]{0,1:T(2,128)S(1)}, f32[4,2,256]{2,1,0:T(2,128)S(1)}) all-reduce(f32[4,2]{0,1:T(2,128)S(1)} %multiply_reduce_fusion, f32[4,2,256]{2,1,0:T(2,128)S(1)} %bitcast.66), channel_id=1, replica_groups=mesh['sp'=8,'tp'=4] {'sp'}, use_global_device_ids=true, to_apply=%region_11.12 | all-reduce | flops 2056 | bytes 16448 | tf_op jit(solution)/shard_map/psum | solution.py:92
  101.7 2.0 fusion.6
  103.7 0.1 reduce_sum.39
  103.8 0.1 copy.53
  103.9 0.1 convolution_bitcast_fusion.1
  104.0 0.0 copy-done.3
  104.0 0.9 abs_maximum_fusion
  104.9 0.1 copy.55
  105.0 2.0 fusion.3
  107.1 0.1 copy.54
  107.1 0.1 copy.52
  107.2 0.1 fusion.17
  107.3 2.0 convolution_convert_fusion
  109.3 10.7 %psum.23 = bf16[4,2048]{1,0:T(4,128)(2,1)} all-reduce(bf16[4,2048]{1,0:T(4,128)(2,1)S(1)} %convolution_convert_fusion), channel_id=1, replica_groups=mesh['sp'=8,'tp'=4] {'tp'}, use_global_device_ids=true, to_apply=%region_12.13 | all-reduce | flops 8192 | bytes 32768 | tf_op jit(solution)/shard_map/psum | solution.py:107
  120.0 11.0 %reduce-scatter.7.cloned.1.call-done = f32[128,2]{1,0:T(8,128)} async-done(((f32[1024,2]{1,0:T(8,128)}), f32[128,2]{1,0:T(8,128)}) %reduce-scatter.7.cloned.1.call-update) | async-done | bytes 1040
  131.0 1.5 copy.67
  132.5 69.4 %reduce-scatter.5.cloned.1.call-done = f32[2,128,256]{2,1,0:T(8,128)} async-done(((f32[2,1024,256]{2,1,0:T(8,128)}), f32[2,128,256]{2,1,0:T(8,128)}) %reduce-scatter.5.cloned.1.call-update) | async-done | bytes 262160 | tf_op jit(solution)/shard_map/reduce_scatter | solution.py:64
  201.9 1.6 convert_element_type.58
  (16 shorter events, 0.2 us)
Async XLA Ops:
  7.2 1.6 copy-start
  7.2 3.1 %copy-start.2 = (f32[2,4,128]{2,1,0:T(4,128)S(1)}, f32[2,4,128]{2,1,0:T(4,128)}, u32[]{:S(2)}) copy-start(f32[2,4,128]{2,1,0:T(4,128)} %param.18) | copy-start | bytes 12292
  7.2 123.8 %reduce-scatter.7.cloned.1.call-start = ((), (), s32[]{:S(2)}) async-start(), calls=%async_computation.3 | async-start | bytes 589824
  41.6 3.3 %copy-start.4 = (bf16[2048,8]{0,1:T(8,128)(2,1)S(1)}, bf16[2048,8]{0,1:T(8,128)(2,1)}, u32[]{:S(2)}) copy-start(bf16[2048,8]{0,1:T(8,128)(2,1)} %param.15) | copy-start | bytes 98308
  66.6 37.5 %copy-start.3 = (f32[4,2]{0,1:T(2,128)}, f32[4,2]{0,1:T(2,128)S(1)}, u32[]{:S(2)}) copy-start(f32[4,2]{0,1:T(2,128)S(1)} %max.30) | copy-start | bytes 100
  71.0 130.9 %reduce-scatter.5.cloned.1.call-start = ((), (), s32[]{:S(2)}) async-start(), calls=%async_computation.2 | async-start | bytes 2359296 | tf_op jit(solution)/shard_map/reduce_scatter | solution.py:64
  76.6 2.9 %copy-start.1 = (bf16[4,2048]{1,0:T(4,128)(2,1)S(1)}, bf16[4,2048]{1,0:T(4,128)(2,1)}, u32[]{:S(2)}) copy-start(bf16[4,2048]{1,0:T(4,128)(2,1)} %param.11) | copy-start | bytes 49156
Sparse Core Ops, SparseCore 0:
  71.1 59.8 reduce-scatter.6
  134.5 67.3 reduce-scatter.4
where the time goes:
time: 211 us; the launch traced here: 210 us
  waiting for transfers between devices  80.4 us (38%)
  blocking collectives  75.4 us (36%)
  matrix products  22.7 us (11%)
  between operations  14.2 us (7%)
  local copies, waits for them, and re-layouts  12.2 us (6%)
  other arithmetic  5.39 us (3%)
    reduce_scatter x1, waiting for transfers between devices, per_device(): lax.psum_scatter(memory_term, 'sp', scatter_dimension=1, tiled=True)  69.4 us
    all_gather x1, blocking collectives, per_device(): lax.all_gather(block_total[None], 'sp', axis=0, tiled=True)  27.9 us
    all_gather x1, blocking collectives, per_device(): lax.all_gather(block_peak[None], 'sp', axis=0, tiled=True)  19 us
    psum x1, blocking collectives, per_device(): query_state, query_norm = lax.psum((numer_slots, denom_slots), 'sp')  17.7 us
    unnamed x3, waiting for transfers between devices  11 us
    psum x1, blocking collectives, per_device(): read = lax.psum(partial_value.astype(jnp.bfloat16), 'tp')  10.7 us
  transfers between devices with their start and end apart: 2, of which 2 were waited for; matrix products, arithmetic and copies ran while one was open for 10% of the time, Pallas kernels for 0%

commit v1 on v0

--- a/solution.py
+++ b/solution.py
@@ -43,7 +43,9 @@
     block_peak = jnp.max(local_score, axis=1)
     totals, peaks = (
         lax.all_gather(block_total[None], "sp", axis=0, tiled=True),
-        lax.all_gather(block_peak[None], "sp", axis=0, tiled=True),
+        jnp.concatenate(
+            lax.all_to_all(jnp.stack([block_peak[None]] * lax.axis_size("sp")), "sp", 0, 0), axis=0
+        ),
     )
     later = jnp.flip(jnp.cumsum(jnp.flip(totals, 0), axis=0), 0) - totals
     prompt_total = jnp.sum(totals, axis=0)

time: 211 us -> 204 us (0.967)
  blocking collectives: 75.4 us -> 57.8 us
  starting transfers between devices: 0.08 us -> 7.39 us
  waiting for transfers between devices: 80.4 us -> 85.4 us
    all_gather x1 -> x0, blocking collectives: 19 us -> none  [per_device(): lax.all_gather(block_peak[None], 'sp', axis=0, tiled=True)]
    all_to_all x0 -> x1, starting transfers between devices: none -> 7.31 us  [per_device(): lax.all_to_all(jnp.stack([block_peak[None]] * lax.axis_size('sp')), 'sp',...]
    unnamed x3, waiting for transfers between devices: 11 us -> 16 us
    psum x1, blocking collectives: 17.7 us -> 20.3 us  [per_device(): query_state, query_norm = lax.psum((numer_slots, denom_slots), 'sp')]
  transfers between devices with their start and end apart: 2 -> 3, of which waited for: 2 -> 2; matrix products, arithmetic and copies ran while one was open for 10% -> 13% of each run, Pallas kernels for 0% -> 0%
where the time goes in v1:
time: 204 us; the launch traced here: 203 us
  waiting for transfers between devices  85.4 us (42%)
  blocking collectives  57.8 us (28%)
  matrix products  21.4 us (10%)
  between operations  14.3 us (7%)
  local copies, waits for them, and re-layouts  12.4 us (6%)
  starting transfers between devices  7.39 us (4%)
  other arithmetic  4.42 us (2%)
    reduce_scatter x1, waiting for transfers between devices, per_device(): lax.psum_scatter(memory_term, 'sp', scatter_dimension=1, tiled=True)  69.4 us
    all_gather x1, blocking collectives, per_device(): lax.all_gather(block_total[None], 'sp', axis=0, tiled=True)  26.6 us
    psum x1, blocking collectives, per_device(): query_state, query_norm = lax.psum((numer_slots, denom_slots), 'sp')  20.3 us
    unnamed x3, waiting for transfers between devices  16 us
    psum x1, blocking collectives, per_device(): read = lax.psum(partial_value.astype(jnp.bfloat16), 'tp')  10.9 us
    all_to_all x1, starting transfers between devices, per_device(): lax.all_to_all(jnp.stack([block_peak[None]] * lax.axis_size('sp')), 'sp',...  7.31 us
    convert_element_type x2, local copies, waits for them, and re-layouts, per_device(): key_heads.astype(jnp.float32) * weight[:, :, :, None]  4.36 us
  transfers between devices with their start and end apart: 3, of which 2 were waited for; matrix products, arithmetic and copies ran while one was open for 13% of the time, Pallas kernels for 0%

profile of v1, /device:TPU:0, one launch (start us, length us, event | category | flops | bytes accessed | tf_op | source)
XLA Modules:
  0.0 203.2 jit_solution(12673208738392232505)
XLA Ops:
  7.2 0.0 copy-start
  7.2 0.0 copy-start.4
  7.2 0.0 copy-start.6
  7.2 0.9 dynamic_slice.10
  8.1 0.7 copy-done
  8.8 1.4 fusion.16
  10.2 0.0 copy-done.4
  10.3 0.1 copy.40
  10.4 0.3 reduce_window_sum.22
  10.7 0.0 copy-done.6
  10.7 0.6 convolution_bitcast_fusion
  11.3 0.2 copy.66
  11.5 0.0 copy-start.1
  11.5 0.1 fusion.13
  11.6 0.1 copy.46
  11.7 0.6 stack.3
  12.3 7.3 %all-to-all-start = ((f32[8,1,4,2]{2,3,1,0:T(2,128)}), f32[8,1,4,2]{2,3,1,0:T(2,128)S(1)}, u32[]{:S(2)}, u32[]{:S(2)}) async-start(f32[8,1,4,2]{2,3,1,0:T(2,128)} %stack.3), calls=%async_computation | async-start | bytes 16384 | tf_op jit(solution)/shard_map/all_to_all | solution.py:47
  19.6 0.0 reduce-scatter.7.cloned.1.call-start
  19.6 26.6 %all-gather = f32[32,1,2]{2,1,0:T(1,128)S(1)} all-gather(f32[4,1,2]{2,1,0:T(1,128)S(1)} %slice.4), channel_id=2, replica_groups=mesh['sp'=8,'tp'=4] {'sp'}, dimensions={0}, use_global_device_ids=true | all-gather | bytes 288 | tf_op jit(solution)/shard_map/all_gather | solution.py:45
  46.2 0.0 copy-start.2
  46.2 3.0 %convolution_convert_fusion.1 = bf16[512,512]{1,0:T(8,128)(2,1)S(1)} fusion(bf16[512,2048]{1,0:T(8,128)(2,1)S(1)} %bitcast.56, bf16[2048,512]{1,0:T(8,128)(2,1)} %param.14), kind=kOutput, calls=%fused_computation.3 | convolution fusion | flops 1074003968 | bytes 4718592 | tf_op jit(solution)/shard_map/dot_general | solution.py:33
  49.2 0.0 copy-done.1
  49.2 0.0 copy-done.2
  49.3 2.3 %fusion.2 = f32[512,512]{1,0:T(8,128)} fusion(bf16[512,2048]{1,0:T(8,128)(2,1)S(1)} %bitcast.53, bf16[2048,512]{1,0:T(8,128)(2,1)S(1)} %copy-done.2), kind=kOutput, calls=%fused_computation.5 | convolution fusion | flops 1074266112 | bytes 5242880 | tf_op jit(solution)/shard_map/dot_general | solution.py:32
  51.5 0.1 copy.64
  51.7 0.9 reshape.81
  52.6 2.9 %reshape.88 = f32[4,128,2,256]{3,2,1,0:T(2,128)} reshape(f32[512,512]{1,0:T(8,128)} %fusion.2) | data formatting | bytes 2097152 | tf_op jit(solution)/shard_map/convert_element_type | solution.py:58
  55.5 1.5 copy.51
  57.0 0.1 copy.72
  57.1 0.0 all-to-all-done
  57.1 0.1 multiply_reduce_fusion.1
  57.2 0.1 copy.49
  57.3 0.1 copy.42
  57.4 1.7 exponential_multiply_fusion
  59.1 1.1 copy.50
  60.2 0.4 convert_reduce_fusion
  60.5 1.1 copy.71
  61.6 0.0 reduce-scatter.7.cloned.1.call-update
  61.6 0.0 copy-start.3
  61.6 0.0 reduce-scatter.5.cloned.1.call-start
  61.7 2.8 %fusion.11 = f32[2,4,256,256]{3,2,1,0:T(8,128)} fusion(bf16[4,128,2,256]{3,2,1,0:T(2,128)(2,1)} %reshape.81, f32[4,128,2,256]{1,3,0,2:T(8,128)S(1)} %copy.51, f32[4,128,2]{1,0,2:T(4,128)S(1)} %copy.50), kind=kOutput, calls=%fused_computation.23 | convolution fusion | flops 134742016 | bytes 3674112 | tf_op jit(solution)/shard_map/sthd,sthe->hsde/dot_general | solution.py:59
  64.5 0.0 reduce-scatter.5.cloned.1.call-update
  64.5 0.0 copy-done.3
  64.5 2.0 convolution_convert_fusion.5
  66.5 2.0 fusion.6
  68.5 0.1 reduce_sum.39
  68.6 0.1 copy.54
  68.7 2.0 fusion.3
  70.7 0.1 convolution_bitcast_fusion.1
  70.8 2.4 %fusion = f32[4,2,1,256]{3,2,1,0:T(1,128)S(1)} fusion(bf16[4,2,256,1]{2,3,1,0:T(2,128)(2,1)S(1)} %reshape.97, f32[2,4,256,256]{3,2,1,0:T(8,128)} %fusion.11), kind=kOutput, calls=%fused_computation.1 | convolution fusion | flops 6291456 | bytes 2109440 | tf_op jit(solution)/shard_map/shd,hsde->she/dot_general | solution.py:92
  73.2 0.1 multiply_reduce_fusion
  73.3 20.3 %all-reduce = (f32[4,2]{0,1:T(2,128)S(1)}, f32[4,2,256]{2,1,0:T(2,128)S(1)}) all-reduce(f32[4,2]{0,1:T(2,128)S(1)} %multiply_reduce_fusion, f32[4,2,256]{2,1,0:T(2,128)S(1)} %bitcast.67), channel_id=1, replica_groups=mesh['sp'=8,'tp'=4] {'sp'}, use_global_device_ids=true, to_apply=%region_11.12 | all-reduce | flops 2056 | bytes 16448 | tf_op jit(solution)/shard_map/psum | solution.py:94
  93.7 0.0 copy-done.5
  93.7 0.9 abs_maximum_fusion
  94.6 0.1 copy.56
  94.7 0.1 copy.55
  94.8 0.1 copy.53
  94.9 0.1 fusion.17
  95.0 2.0 convolution_convert_fusion
  97.0 10.9 %psum.23 = bf16[4,2048]{1,0:T(4,128)(2,1)} all-reduce(bf16[4,2048]{1,0:T(4,128)(2,1)S(1)} %convolution_convert_fusion), channel_id=1, replica_groups=mesh['sp'=8,'tp'=4] {'tp'}, use_global_device_ids=true, to_apply=%region_12.13 | all-reduce | flops 8192 | bytes 32768 | tf_op jit(solution)/shard_map/psum | solution.py:109
  107.8 16.0 %reduce-scatter.7.cloned.1.call-done = f32[128,2]{1,0:T(8,128)} async-done(((f32[1024,2]{1,0:T(8,128)}), f32[128,2]{1,0:T(8,128)}) %reduce-scatter.7.cloned.1.call-update) | async-done | bytes 1040
  123.8 1.5 copy.70
  125.3 69.4 %reduce-scatter.5.cloned.1.call-done = f32[2,128,256]{2,1,0:T(8,128)} async-done(((f32[2,1024,256]{2,1,0:T(8,128)}), f32[2,128,256]{2,1,0:T(8,128)}) %reduce-scatter.5.cloned.1.call-update) | async-done | bytes 262160 | tf_op jit(solution)/shard_map/reduce_scatter | solution.py:66
  194.7 1.6 convert_element_type.58
  (17 shorter events, 0.2 us)
Async XLA Ops:
  7.2 1.6 copy-start
  7.2 3.1 %copy-start.4 = (f32[2,4,128]{2,1,0:T(4,128)S(1)}, f32[2,4,128]{2,1,0:T(4,128)}, u32[]{:S(2)}) copy-start(f32[2,4,128]{2,1,0:T(4,128)} %param.18) | copy-start | bytes 12292
  7.2 3.5 %copy-start.6 = (bf16[2048,8]{0,1:T(8,128)(2,1)S(1)}, bf16[2048,8]{0,1:T(8,128)(2,1)}, u32[]{:S(2)}) copy-start(bf16[2048,8]{0,1:T(8,128)(2,1)} %param.15) | copy-start | bytes 98308
  11.5 37.7 %copy-start.1 = (f32[512,2]{1,0:T(8,128)}, f32[512,2]{1,0:T(8,128)S(1)}, u32[]{:S(2)}) copy-start(f32[512,2]{1,0:T(8,128)S(1)} %copy.66) | copy-start | bytes 12292
  12.3 44.8 %all-to-all-start = ((f32[8,1,4,2]{2,3,1,0:T(2,128)}), f32[8,1,4,2]{2,3,1,0:T(2,128)S(1)}, u32[]{:S(2)}, u32[]{:S(2)}) async-start(f32[8,1,4,2]{2,3,1,0:T(2,128)} %stack.3), calls=%async_computation | async-start | bytes 16384 | tf_op jit(solution)/shard_map/all_to_all | solution.py:47
  19.6 104.2 %reduce-scatter.7.cloned.1.call-start = ((), (), s32[]{:S(2)}) async-start(), calls=%async_computation.4 | async-start | bytes 589824
  46.2 3.0 %copy-start.2 = (bf16[2048,512]{1,0:T(8,128)(2,1)S(1)}, bf16[2048,512]{1,0:T(8,128)(2,1)}, u32[]{:S(2)}) copy-start(bf16[2048,512]{1,0:T(8,128)(2,1)} %param.13) | copy-start | bytes 6291460
  57.2 36.5 %copy-start.5 = (f32[4,2]{0,1:T(2,128)}, f32[4,2]{0,1:T(2,128)S(1)}, u32[]{:S(2)}) copy-start(f32[4,2]{0,1:T(2,128)S(1)} %max.30) | copy-start | bytes 100
  61.6 2.9 %copy-start.3 = (bf16[4,2048]{1,0:T(4,128)(2,1)S(1)}, bf16[4,2048]{1,0:T(4,128)(2,1)}, u32[]{:S(2)}) copy-start(bf16[4,2048]{1,0:T(4,128)(2,1)} %param.11) | copy-start | bytes 49156
  61.6 133.1 %reduce-scatter.5.cloned.1.call-start = ((), (), s32[]{:S(2)}) async-start(), calls=%async_computation.3 | async-start | bytes 2359296 | tf_op jit(solution)/shard_map/reduce_scatter | solution.py:66
Sparse Core Ops, SparseCore 0:
  61.7 62.0 reduce-scatter.6
  127.3 67.3 reduce-scatter.4
